TPU v7x, 32 devices: a whole 2x2x4 slice. The times are simulated.
32 devices in a mesh: sp: 16 (over z, y, x), tp: 2 (over core).
Axes of the slice: x: 2, y: 2, z: 4, core: 2. Of those that a mesh axis runs over, the one named last changes fastest.
Arguments:
- tokens: bfloat16 [6144, 2048], P('sp', 'tp'), may hold values from -6 to 6
- input_gain: float32 [2048], replicated, may hold values from 0.1 to 1.9
- query_weight: bfloat16 [2048, 1024], P(None, 'tp'), may hold values from -0.5 to 0.5
- query_rot_weight: bfloat16 [2048, 512], P(None, 'tp'), may hold values from -0.125 to 0.125
- kv_down: bfloat16 [2048, 256], replicated, may hold values from -0.5 to 0.5
- rot_down: bfloat16 [2048, 32], replicated, may hold values from -0.125 to 0.125
- kv_gain: float32 [256], replicated, may hold values from 0.1 to 1.9
- key_up: bfloat16 [256, 1024], P(None, 'tp'), may hold values from -0.5 to 0.5
- value_up: bfloat16 [256, 1024], P(None, 'tp'), may hold values from -4 to 4
- conv_value_weight: bfloat16 [2048, 1024], P(None, 'tp'), may hold values from -0.125 to 0.125
- conv_gate_weight: bfloat16 [2048, 1024], P(None, 'tp'), may hold values from -0.125 to 0.125
- conv_taps: float32 [31, 1024], P(None, 'tp'), may hold values from -8 to 8
- conv_ln_gain: float32 [1024], P('tp'), may hold values from 0.1 to 1.9
- conv_ln_bias: float32 [1024], P('tp'), may hold values from -3 to 3
- att_out_gain: float32 [1024], P('tp'), may hold values from 0.1 to 1.9
- conv_out_gain: float32 [1024], P('tp'), may hold values from 0.1 to 1.9
- att_out_weight: bfloat16 [1024, 2048], P('tp'), may hold values from -0.125 to 0.125
- conv_out_weight: bfloat16 [1024, 2048], P('tp'), may hold values from -0.125 to 0.125
Outputs:
- mixed: bfloat16 [6144, 2048], P('sp', 'tp')
All inputs are finite; a program needn't handle non-finite values.
Results may differ from a plain program's by a relative error of at most 0.017.
Values may be sent and summed in bfloat16 or wider, within the bound.
No kernel may reach another device: no remote copies, remote signals or barrier semaphores. Data moves between devices by JAX's collectives and lax.ppermute only.
A program may use at most 128 MiB of HBM per device.

v0:
```python
import math

import jax
import jax.numpy as jnp
from jax import lax
from jax.sharding import PartitionSpec as P

D_MODEL = 2048
NOPE_DIM = 64
ROT_DIM = 32
VALUE_DIM = 64
CONV_CH = 1024
KERNEL = 31
ATT_WIDTH = 1024


norm_eps = 1e-06
far_below = -1e30
rope_base = 10000.0


def shifted(block, axis, distance):
    devices = range(lax.axis_size(axis))
    route = [(i - distance, i) for i in devices if i - distance in devices]
    return lax.ppermute(block, axis, route)


def rotary_tables(positions, half_dim):
    frequency = rope_base ** (-jnp.arange(half_dim, dtype=jnp.float32) / half_dim)
    angles = positions.astype(jnp.float32)[:, None] * frequency[None, :]
    return (jnp.cos(angles), jnp.sin(angles))


def rotate_half(values, cos_table, sine_table):
    half_dim = cos_table.shape[-1]
    front_half = values[..., :half_dim]
    back_half = values[..., half_dim:]
    return jnp.concatenate(
        [
            front_half * cos_table - back_half * sine_table,
            back_half * cos_table + front_half * sine_table,
        ],
        axis=-1,
    )


def shards(
    tokens,
    input_gain,
    query_weight,
    query_rot_weight,
    kv_down,
    rot_down,
    kv_gain,
    key_up,
    value_up,
    conv_value_weight,
    conv_gate_weight,
    conv_taps,
    conv_ln_gain,
    conv_ln_bias,
    att_out_gain,
    conv_out_gain,
    att_out_weight,
    conv_out_weight,
):
    tok_rows = tokens.shape[0]
    heads_here = key_up.shape[1] // NOPE_DIM
    chan_here = conv_taps.shape[1]
    weight_list = (
        query_weight,
        query_rot_weight,
        kv_down,
        rot_down,
        conv_value_weight,
        conv_gate_weight,
    )
    wide_part = lax.all_gather(tokens, "tp", axis=1, tiled=True).astype(jnp.float32)
    scaled = (wide_part * input_gain[None, :]).astype(jnp.bfloat16)

    def add_product(weight):
        return jnp.dot(scaled, weight, preferred_element_type=jnp.float32)

    summed = tuple((add_product(weight) for weight in weight_list))
    q_acc, qrot_acc, latent_raw, rot_acc, value_acc, gate_acc, square_sum = summed + (
        jnp.sum(wide_part * wide_part, axis=1),
    )
    row_scale = lax.rsqrt(square_sum / D_MODEL + norm_eps)[:, None]
    positions = lax.axis_index("sp") * tok_rows + jnp.arange(tok_rows, dtype=jnp.int32)
    cos_table, sine_table = rotary_tables(positions, ROT_DIM // 2)
    queries = (q_acc * row_scale).astype(jnp.bfloat16).reshape(tok_rows, heads_here, NOPE_DIM)
    query_rot = rotate_half(
        (qrot_acc * row_scale).reshape(tok_rows, heads_here, ROT_DIM),
        cos_table[:, None, :],
        sine_table[:, None, :],
    ).astype(jnp.bfloat16)
    latent = (
        latent_raw
        * lax.rsqrt(jnp.mean(latent_raw * latent_raw, axis=1, keepdims=True) + norm_eps)
        * kv_gain[None, :]
    ).astype(jnp.bfloat16)
    key_rot = rotate_half(rot_acc * row_scale, cos_table, sine_table).astype(jnp.bfloat16)
    gated_input = (value_acc * row_scale * jax.nn.sigmoid(gate_acc * row_scale)).astype(
        jnp.bfloat16
    )
    query_end = (lax.axis_index("sp") + 1) * tok_rows
    inv_scale = 1.0 / math.sqrt(NOPE_DIM + ROT_DIM)

    def attend(carried, key_block, rot_block, value_block, key_offset):
        run_max, run_sum, run_acc = carried
        block_len = key_block.shape[0]
        scores = (
            jnp.einsum("qhd,khd->hqk", queries, key_block, preferred_element_type=jnp.float32)
            + jnp.einsum("qhd,kd->hqk", query_rot, rot_block, preferred_element_type=jnp.float32)
        ) * inv_scale
        key_pos = key_offset + jnp.arange(block_len, dtype=jnp.int32)
        visible = (key_pos[None, :] <= positions[:, None])[None]
        new_max = jnp.maximum(run_max, jnp.max(jnp.where(visible, scores, far_below), axis=2))
        exp_scores = jnp.where(visible, jnp.exp(scores - new_max[:, :, None]), 0.0)
        shrink = jnp.exp(run_max - new_max)
        run_sum = run_sum * shrink + jnp.sum(exp_scores, axis=2)
        run_acc = run_acc * shrink.T[:, :, None] + jnp.einsum(
            "hqk,khd->qhd",
            exp_scores.astype(jnp.bfloat16),
            value_block,
            preferred_element_type=jnp.float32,
        )
        return (new_max, run_sum, run_acc)

    def expand_latent(sliced):
        lat_block, rot_block = sliced
        key_block = (
            jnp.dot(lat_block, key_up, preferred_element_type=jnp.float32)
            .astype(jnp.bfloat16)
            .reshape(-1, heads_here, NOPE_DIM)
        )
        value_block = (
            jnp.dot(lat_block, value_up, preferred_element_type=jnp.float32)
            .astype(jnp.bfloat16)
            .reshape(-1, heads_here, VALUE_DIM)
        )
        return (key_block, value_block, rot_block)

    def square_rows(matrix):
        wide_rows = matrix.astype(jnp.float32)
        return jnp.sum(wide_rows * wide_rows, axis=1)

    start_state = (
        jnp.full((heads_here, tok_rows), far_below, jnp.float32),
        jnp.zeros((heads_here, tok_rows), jnp.float32),
        jnp.zeros((tok_rows, heads_here, VALUE_DIM), jnp.float32),
    )
    pieces = (
        lax.all_gather(latent, "sp", axis=0, tiled=True),
        lax.all_gather(key_rot, "sp", axis=0, tiled=True),
    )
    piece_rows = pieces[0].shape[0]
    step_len = math.gcd(piece_rows, 512)

    def visit_block(running, block_idx):
        start_row = block_idx * step_len
        sliced = tuple(
            (lax.dynamic_slice_in_dim(member, start_row, step_len, 0) for member in pieces)
        )

        def compute(current):
            key_block, value_block, rot_block = expand_latent(sliced)
            return attend(current, key_block, rot_block, value_block, start_row)

        return (lax.cond(start_row < query_end, compute, lambda current: current, running), None)

    final_state = lax.scan(
        visit_block, start_state, jnp.arange(piece_rows // step_len, dtype=jnp.int32)
    )[0]
    run_max, run_sum, run_acc = final_state
    attended = (
        (run_acc / run_sum.T[:, :, None])
        .astype(jnp.bfloat16)
        .reshape(tok_rows, heads_here * VALUE_DIM)
    )
    att_sq = lax.psum(square_rows(attended), "tp")
    rim_rows = shifted(gated_input[tok_rows - (KERNEL - 1) :], "sp", 1)
    padded = jnp.concatenate([rim_rows, gated_input], axis=0)
    conv_out = jnp.zeros((tok_rows, chan_here), jnp.float32)
    for tap_idx in range(KERNEL):
        conv_out = conv_out + conv_taps[tap_idx][None, :] * padded[
            tap_idx : tap_idx + tok_rows
        ].astype(jnp.float32)
    moment_one, moment_two = lax.psum(
        (jnp.sum(conv_out, axis=1), jnp.sum(conv_out * conv_out, axis=1)), "tp"
    )
    mean_val = moment_one / CONV_CH
    spread = moment_two / CONV_CH - mean_val * mean_val
    normed = (conv_out - mean_val[:, None]) * lax.rsqrt(spread + norm_eps)[:, None]
    swished = jax.nn.silu(normed * conv_ln_gain[None, :] + conv_ln_bias[None, :])
    conv_sq = lax.psum(square_rows(swished), "tp")
    att_mixed = (
        attended.astype(jnp.float32)
        * lax.rsqrt(att_sq / ATT_WIDTH + norm_eps)[:, None]
        * att_out_gain[None, :]
    ).astype(jnp.bfloat16)
    conv_mixed = (
        swished * lax.rsqrt(conv_sq / CONV_CH + norm_eps)[:, None] * conv_out_gain[None, :]
    ).astype(jnp.bfloat16)
    contract = (((0,), (1,)), ((), ()))
    feature_rows = lax.psum_scatter(
        (
            lax.dot_general(att_out_weight, att_mixed, contract, preferred_element_type=jnp.float32)
            + lax.dot_general(
                conv_out_weight, conv_mixed, contract, preferred_element_type=jnp.float32
            )
        ).astype(jnp.bfloat16),
        "tp",
        scatter_dimension=0,
        tiled=True,
    ).astype(jnp.float32)
    return feature_rows.T.astype(jnp.bfloat16)


def solution(mesh):
    return jax.shard_map(
        shards,
        mesh=mesh,
        in_specs=(
            P("sp", "tp"),
            P(),
            P(None, "tp"),
            P(None, "tp"),
            P(),
            P(),
            P(),
            P(None, "tp"),
            P(None, "tp"),
            P(None, "tp"),
            P(None, "tp"),
            P(None, "tp"),
            P("tp"),
            P("tp"),
            P("tp"),
            P("tp"),
            P("tp", None),
            P("tp", None),
        ),
        out_specs=P("sp", "tp"),
        check_vma=False,
    )
```

profile of v0, /device:TPU:31, one launch (start us, length us, event | category | flops | bytes accessed | tf_op | source)
XLA Modules:
  0.0 247.3 jit_solution(14839390345446647439)
XLA Ops:
  7.3 13.0 %all-gather.3.cloned.1.call-done = bf16[384,2048]{1,0:T(8,128)(2,1)} async-done(((bf16[384,1024]{1,0:T(8,128)(2,1)}), bf16[384,2048]{1,0:T(8,128)(2,1)}) %all-gather.3.cloned.1.call-update) | async-done | bytes 1572880 | tf_op jit(solution)/shard_map/all_gather | solution.py:78
  20.3 2.5 %multiply_reduce_fusion.3 = (f32[384]{0:T(512)S(1)}, f32[384,256]{0,1:T(8,128)S(1)}) fusion(bf16[2048,256]{1,0:T(8,128)(2,1)} %param.26, bf16[384,2048]{1,0:T(8,128)(2,1)} %all-gather.3.cloned.1.call-done, f32[2048]{0:T(1024)} %param.23), kind=kOutput, calls=%fused_computation.128 | convolution fusion | flops 405208704 | bytes 3024384 | tf_op jit(solution)/shard_map/dot_general | solution.py:82
  26.3 3.3 %fusion.33 = f32[384,512]{1,0:T(8,128)S(1)} fusion(bf16[2048,512]{1,0:T(8,128)(2,1)} %param.32, bf16[384,2048]{1,0:T(8,128)(2,1)} %all-gather.3.cloned.1.call-done, f32[2048]{0:T(1024)S(1)} %copy-done.16, f32[384]{0:T(512)S(1)} %add_rsqrt_fusion.3), kind=kOutput, calls=%fused_computation.72 | convolution fusion | flops 808452096 | bytes 4466176 | tf_op jit(solution)/shard_map/dot_general | solution.py:82
  32.9 33.7 %all_gather.11 = bf16[6144,32]{0,1:T(8,128)(2,1)} all-gather(bf16[384,32]{0,1:T(8,128)(2,1)S(1)} %pad_maximum_fusion.2), channel_id=1, replica_groups=mesh['sp'=16,'tp'=2] {'sp'}, dimensions={0}, use_global_device_ids=true | all-gather | bytes 417792 | tf_op jit(solution)/shard_map/all_gather | solution.py:155
  68.7 14.7 %fusion.77 = (f32[384]{0:T(512)}, f32[384]{0:T(512)}, f32[384,512]{1,0:T(8,128)S(1)}) fusion(bf16[384,512]{1,0:T(8,128)(2,1)} %copy-done.5, f32[512]{0:T(512)S(1)} %bitcast.93, bf16[30,512]{1,0:T(8,128)(2,1)S(1)} %collective-permute-done, f32[512]{0:T(512)S(1)} %bitcast.94, f32[512]{0:T(512)} %bitcast.96, f32[512]{0:T(512)} %bitcast.97, f32[512]{0:T(512)} %bitcast.98, ...), kind=kLoop, calls=%fused_computation.145 | loop fusion | flops 36371712 | bytes 1276928 | tf_op jit(solution)/shard_map/reduce_sum | solution.py:190
  83.4 9.8 %all-reduce.1 = (f32[384]{0:T(512)S(1)}, f32[384]{0:T(512)S(1)}) all-reduce(f32[384]{0:T(512)} %get-tuple-element.271, f32[384]{0:T(512)} %get-tuple-element.270), channel_id=1, replica_groups=mesh['sp'=16,'tp'=2] {'tp'}, use_global_device_ids=true, to_apply=%region_13.14 | all-reduce | flops 768 | bytes 6144 | tf_op jit(solution)/shard_map/psum | solution.py:189
  94.4 4.7 %copy.24 = bf16[6144,256]{1,0:T(8,128)(2,1)} copy(bf16[6144,256]{0,1:T(8,128)(2,1)} %all-gather.5.cloned.1.call-done) | data formatting | bytes 6291456
  99.1 122.8 %while.15 = (s32[]{:T(128)}, f32[8,384]{1,0:T(8,128)S(1)}, f32[8,384]{1,0:T(8,128)S(1)}, f32[384,8,64]{0,2,1:T(8,128)S(1)}, s32[12]{0:T(128)S(1)}, /*index=5*/s3...) while((s32[]{:T(128)}, f32[8,384]{1,0:T(8,128)S(1)}, ...), condition=%wide.region_7.8_spmd.clone, body=%wide.region_2.7_spmd.clone.sunk | while | flops 788604800 | bytes 38840728 | solution.py:172
  100.4 9.0 %conditional.3 = ((f32[8,384]{1,0:T(8,128)S(1)}, f32[8,384]{1,0:T(8,128)S(1)}, f32[384,8,64]{0,2,1:T(8,128)S(1)})) conditional(s32[]{:T(128)} %convert_element_type.326, (f32[8,384]{1,0:T(8,128)S(1)}, f32[8,384]{1,0:T(8,128)S(1)}, f32[384,8,64]{0,2,1:T(8,128)S(1)}) %tuple.85, (s32[]{:T(128)}, s32[]{:T(128)}, bf16[6144,256]{1,0:T(8,128)(2,1)}, ...), branch_computations={%region_3.3_spmd, %region_4.6_spmd} | conditional | flops 788604800 | bytes 38838896 | solution.py:170
  101.8 1.9 fusion.18
  110.6 9.0 %conditional.3 = ((f32[8,384]{1,0:T(8,128)S(1)}, f32[8,384]{1,0:T(8,128)S(1)}, f32[384,8,64]{0,2,1:T(8,128)S(1)})) conditional(s32[]{:T(128)} %convert_element_type.326, (f32[8,384]{1,0:T(8,128)S(1)}, f32[8,384]{1,0:T(8,128)S(1)}, f32[384,8,64]{0,2,1:T(8,128)S(1)}) %tuple.85, (s32[]{:T(128)}, s32[]{:T(128)}, bf16[6144,256]{1,0:T(8,128)(2,1)}, ...), branch_computations={%region_3.3_spmd, %region_4.6_spmd} | conditional | flops 788604800 | bytes 38838896 | solution.py:170
  120.9 9.0 %conditional.3 = ((f32[8,384]{1,0:T(8,128)S(1)}, f32[8,384]{1,0:T(8,128)S(1)}, f32[384,8,64]{0,2,1:T(8,128)S(1)})) conditional(s32[]{:T(128)} %convert_element_type.326, (f32[8,384]{1,0:T(8,128)S(1)}, f32[8,384]{1,0:T(8,128)S(1)}, f32[384,8,64]{0,2,1:T(8,128)S(1)}) %tuple.85, (s32[]{:T(128)}, s32[]{:T(128)}, bf16[6144,256]{1,0:T(8,128)(2,1)}, ...), branch_computations={%region_3.3_spmd, %region_4.6_spmd} | conditional | flops 788604800 | bytes 38838896 | solution.py:170
  131.1 9.0 %conditional.3 = ((f32[8,384]{1,0:T(8,128)S(1)}, f32[8,384]{1,0:T(8,128)S(1)}, f32[384,8,64]{0,2,1:T(8,128)S(1)})) conditional(s32[]{:T(128)} %convert_element_type.326, (f32[8,384]{1,0:T(8,128)S(1)}, f32[8,384]{1,0:T(8,128)S(1)}, f32[384,8,64]{0,2,1:T(8,128)S(1)}) %tuple.85, (s32[]{:T(128)}, s32[]{:T(128)}, bf16[6144,256]{1,0:T(8,128)(2,1)}, ...), branch_computations={%region_3.3_spmd, %region_4.6_spmd} | conditional | flops 788604800 | bytes 38838896 | solution.py:170
  141.3 9.0 %conditional.3 = ((f32[8,384]{1,0:T(8,128)S(1)}, f32[8,384]{1,0:T(8,128)S(1)}, f32[384,8,64]{0,2,1:T(8,128)S(1)})) conditional(s32[]{:T(128)} %convert_element_type.326, (f32[8,384]{1,0:T(8,128)S(1)}, f32[8,384]{1,0:T(8,128)S(1)}, f32[384,8,64]{0,2,1:T(8,128)S(1)}) %tuple.85, (s32[]{:T(128)}, s32[]{:T(128)}, bf16[6144,256]{1,0:T(8,128)(2,1)}, ...), branch_computations={%region_3.3_spmd, %region_4.6_spmd} | conditional | flops 788604800 | bytes 38838896 | solution.py:170
  151.5 9.0 %conditional.3 = ((f32[8,384]{1,0:T(8,128)S(1)}, f32[8,384]{1,0:T(8,128)S(1)}, f32[384,8,64]{0,2,1:T(8,128)S(1)})) conditional(s32[]{:T(128)} %convert_element_type.326, (f32[8,384]{1,0:T(8,128)S(1)}, f32[8,384]{1,0:T(8,128)S(1)}, f32[384,8,64]{0,2,1:T(8,128)S(1)}) %tuple.85, (s32[]{:T(128)}, s32[]{:T(128)}, bf16[6144,256]{1,0:T(8,128)(2,1)}, ...), branch_computations={%region_3.3_spmd, %region_4.6_spmd} | conditional | flops 788604800 | bytes 38838896 | solution.py:170
  161.8 9.0 %conditional.3 = ((f32[8,384]{1,0:T(8,128)S(1)}, f32[8,384]{1,0:T(8,128)S(1)}, f32[384,8,64]{0,2,1:T(8,128)S(1)})) conditional(s32[]{:T(128)} %convert_element_type.326, (f32[8,384]{1,0:T(8,128)S(1)}, f32[8,384]{1,0:T(8,128)S(1)}, f32[384,8,64]{0,2,1:T(8,128)S(1)}) %tuple.85, (s32[]{:T(128)}, s32[]{:T(128)}, bf16[6144,256]{1,0:T(8,128)(2,1)}, ...), branch_computations={%region_3.3_spmd, %region_4.6_spmd} | conditional | flops 788604800 | bytes 38838896 | solution.py:170
  172.0 9.0 %conditional.3 = ((f32[8,384]{1,0:T(8,128)S(1)}, f32[8,384]{1,0:T(8,128)S(1)}, f32[384,8,64]{0,2,1:T(8,128)S(1)})) conditional(s32[]{:T(128)} %convert_element_type.326, (f32[8,384]{1,0:T(8,128)S(1)}, f32[8,384]{1,0:T(8,128)S(1)}, f32[384,8,64]{0,2,1:T(8,128)S(1)}) %tuple.85, (s32[]{:T(128)}, s32[]{:T(128)}, bf16[6144,256]{1,0:T(8,128)(2,1)}, ...), branch_computations={%region_3.3_spmd, %region_4.6_spmd} | conditional | flops 788604800 | bytes 38838896 | solution.py:170
  182.2 9.0 %conditional.3 = ((f32[8,384]{1,0:T(8,128)S(1)}, f32[8,384]{1,0:T(8,128)S(1)}, f32[384,8,64]{0,2,1:T(8,128)S(1)})) conditional(s32[]{:T(128)} %convert_element_type.326, (f32[8,384]{1,0:T(8,128)S(1)}, f32[8,384]{1,0:T(8,128)S(1)}, f32[384,8,64]{0,2,1:T(8,128)S(1)}) %tuple.85, (s32[]{:T(128)}, s32[]{:T(128)}, bf16[6144,256]{1,0:T(8,128)(2,1)}, ...), branch_computations={%region_3.3_spmd, %region_4.6_spmd} | conditional | flops 788604800 | bytes 38838896 | solution.py:170
  192.5 9.0 %conditional.3 = ((f32[8,384]{1,0:T(8,128)S(1)}, f32[8,384]{1,0:T(8,128)S(1)}, f32[384,8,64]{0,2,1:T(8,128)S(1)})) conditional(s32[]{:T(128)} %convert_element_type.326, (f32[8,384]{1,0:T(8,128)S(1)}, f32[8,384]{1,0:T(8,128)S(1)}, f32[384,8,64]{0,2,1:T(8,128)S(1)}) %tuple.85, (s32[]{:T(128)}, s32[]{:T(128)}, bf16[6144,256]{1,0:T(8,128)(2,1)}, ...), branch_computations={%region_3.3_spmd, %region_4.6_spmd} | conditional | flops 788604800 | bytes 38838896 | solution.py:170
  202.7 9.0 %conditional.3 = ((f32[8,384]{1,0:T(8,128)S(1)}, f32[8,384]{1,0:T(8,128)S(1)}, f32[384,8,64]{0,2,1:T(8,128)S(1)})) conditional(s32[]{:T(128)} %convert_element_type.326, (f32[8,384]{1,0:T(8,128)S(1)}, f32[8,384]{1,0:T(8,128)S(1)}, f32[384,8,64]{0,2,1:T(8,128)S(1)}) %tuple.85, (s32[]{:T(128)}, s32[]{:T(128)}, bf16[6144,256]{1,0:T(8,128)(2,1)}, ...), branch_computations={%region_3.3_spmd, %region_4.6_spmd} | conditional | flops 788604800 | bytes 38838896 | solution.py:170
  212.9 8.9 %conditional.3 = ((f32[8,384]{1,0:T(8,128)S(1)}, f32[8,384]{1,0:T(8,128)S(1)}, f32[384,8,64]{0,2,1:T(8,128)S(1)})) conditional(s32[]{:T(128)} %convert_element_type.326, (f32[8,384]{1,0:T(8,128)S(1)}, f32[8,384]{1,0:T(8,128)S(1)}, f32[384,8,64]{0,2,1:T(8,128)S(1)}) %tuple.85, (s32[]{:T(128)}, s32[]{:T(128)}, bf16[6144,256]{1,0:T(8,128)(2,1)}, ...), branch_computations={%region_3.3_spmd, %region_4.6_spmd} | conditional | flops 788604800 | bytes 38838896 | solution.py:170
  222.9 2.5 all-reduce
  227.9 2.5 fusion.28
  230.4 10.4 %reduce-scatter.2.cloned.1.call-done = bf16[1024,384]{0,1:T(8,128)(2,1)} async-done(((bf16[2048,384]{0,1:T(8,128)(2,1)}), bf16[1024,384]{0,1:T(8,128)(2,1)}) %reduce-scatter.2.cloned.1.call-update) | async-done | bytes 786448 | tf_op jit(solution)/shard_map/reduce_scatter | solution.py:206
  (262 shorter events, 125.3 us)
Async XLA Ops:
  6.5 220.3 %copy-start = (bf16[512,2048]{1,0:T(8,128)(2,1)S(1)}, bf16[512,2048]{1,0:T(8,128)(2,1)}, u32[]{:S(2)}) copy-start(bf16[512,2048]{1,0:T(8,128)(2,1)} %param.38) | copy-start | bytes 6291460
  6.5 16.3 %copy-start.10 = (f32[256]{0:T(256)S(1)}, f32[256]{0:T(256)}, u32[]{:S(2)}) copy-start(f32[256]{0:T(256)} %param.28) | copy-start | bytes 3076
  6.5 17.2 %copy-start.6 = (f32[31,512]{1,0:T(8,128)S(1)}, f32[31,512]{1,0:T(8,128)}, u32[]{:S(2)}) copy-start(f32[31,512]{1,0:T(8,128)} %param.33) | copy-start | bytes 190468
  6.5 13.8 %all-gather.3.cloned.1.call-start = ((), (), s32[]{:S(2)}) async-start(), calls=%async_computation.1 | async-start | bytes 2359296 | tf_op jit(solution)/shard_map/all_gather | solution.py:78
  7.3 19.0 %copy-start.16 = (f32[2048]{0:T(1024)S(1)}, f32[2048]{0:T(1024)}, u32[]{:S(2)}) copy-start(f32[2048]{0:T(1024)} %param.23) | copy-start | bytes 24580
  7.3 87.1 %all-gather.5.cloned.1.call-start = ((), (), s32[]{:S(2)}) async-start(), calls=%async_computation.2 | async-start | bytes 3342336 | tf_op jit(solution)/shard_map/all_gather | solution.py:154
  23.7 217.1 %reduce-scatter.2.cloned.1.call-start = ((), (), s32[]{:S(2)}) async-start(), calls=%async_computation.3 | async-start | bytes 2359296 | tf_op jit(solution)/shard_map/reduce_scatter | solution.py:206
  26.3 3.4 %copy-start.4 = (bf16[384,2048]{1,0:T(8,128)(2,1)S(1)}, bf16[384,2048]{1,0:T(8,128)(2,1)}, u32[]{:S(2)}) copy-start(bf16[384,2048]{1,0:T(8,128)(2,1)} %all-gather.3.cloned.1.call-done) | copy-start | bytes 4718596
  26.3 3.4 %copy-start.11 = (bf16[2048,512]{1,0:T(8,128)(2,1)S(1)}, bf16[2048,512]{1,0:T(8,128)(2,1)}, u32[]{:S(2)}) copy-start(bf16[2048,512]{1,0:T(8,128)(2,1)} %param.31) | copy-start | bytes 6291460
  29.6 2.5 %copy-start.15 = (bf16[2048,32]{0,1:T(8,128)(2,1)S(1)}, bf16[2048,32]{0,1:T(8,128)(2,1)}, u32[]{:S(2)}) copy-start(bf16[2048,32]{0,1:T(8,128)(2,1)} %param.27) | copy-start | bytes 393220
  29.7 37.0 %copy-start.14 = (bf16[2048,256]{1,0:T(8,128)(2,1)S(1)}, bf16[2048,256]{1,0:T(8,128)(2,1)}, u32[]{:S(2)}) copy-start(bf16[2048,256]{1,0:T(8,128)(2,1)} %param.25) | copy-start | bytes 3145732
  30.7 36.8 %copy-start.5 = (bf16[384,512]{1,0:T(8,128)(2,1)}, bf16[384,512]{1,0:T(8,128)(2,1)S(1)}, u32[]{:S(2)}) copy-start(bf16[384,512]{1,0:T(8,128)(2,1)S(1)} %fusion.35) | copy-start | bytes 1179652
  30.7 36.8 %copy-start.12 = (bf16[2048,512]{1,0:T(8,128)(2,1)S(1)}, bf16[2048,512]{1,0:T(8,128)(2,1)}, u32[]{:S(2)}) copy-start(bf16[2048,512]{1,0:T(8,128)(2,1)} %param.24) | copy-start | bytes 6291460
  30.7 38.0 %collective-permute-start = (bf16[30,512]{1,0:T(8,128)(2,1)S(1)}, bf16[30,512]{1,0:T(8,128)(2,1)S(1)}, u32[]{:S(2)}, u32[]{:S(2)}) collective-permute-start(bf16[30,512]{1,0:T(8,128)(2,1)S(1)} %slice.268), channel_id=1, source_target_pairs={{0,2},{2,4},{4,6},{6,8},{8,10},{10,12},{12,14},{14,16},{16,18},{18... | collective-permute-start | bytes 92168 | tf_op jit(solution)/shard_map/ppermute | solution.py:25
  83.4 15.6 %copy-start.2 = (f32[384,512]{1,0:T(8,128)}, f32[384,512]{1,0:T(8,128)S(1)}, u32[]{:S(2)}) copy-start(f32[384,512]{1,0:T(8,128)S(1)} %get-tuple-element.304) | copy-start | bytes 2359300
  99.1 126.2 %copy-start.7 = (f32[512]{0:T(512)S(1)}, f32[512]{0:T(512)}, u32[]{:S(2)}) copy-start(f32[512]{0:T(512)} %param.36) | copy-start | bytes 6148
  144.8 1.6 copy-start.1
  155.0 1.6 copy-start.1
  165.3 1.6 copy-start.1
  225.3 2.5 %copy-start.3 = (f32[384,512]{1,0:T(8,128)S(1)}, f32[384,512]{1,0:T(8,128)}, u32[]{:S(2)}) copy-start(f32[384,512]{1,0:T(8,128)} %copy-done.2) | copy-start | bytes 2359300
  225.3 2.5 %copy-start.8 = (f32[512]{0:T(512)S(1)}, f32[512]{0:T(512)}, u32[]{:S(2)}) copy-start(f32[512]{0:T(512)} %param.35) | copy-start | bytes 6148
  225.3 2.5 %copy-start.9 = (f32[512]{0:T(512)S(1)}, f32[512]{0:T(512)}, u32[]{:S(2)}) copy-start(f32[512]{0:T(512)} %param.34) | copy-start | bytes 6148
  225.4 2.5 %copy-start.13 = (bf16[512,2048]{1,0:T(8,128)(2,1)S(1)}, bf16[512,2048]{1,0:T(8,128)(2,1)}, u32[]{:S(2)}) copy-start(bf16[512,2048]{1,0:T(8,128)(2,1)} %param.39) | copy-start | bytes 6291460
  225.4 2.5 %copy-start.17 = (f32[512]{0:T(512)S(1)}, f32[512]{0:T(512)}, u32[]{:S(2)}) copy-start(f32[512]{0:T(512)} %param.37) | copy-start | bytes 6148
  (9 other events, 14.6 us)
Sparse Core Ops, SparseCore 0:
  8.9 11.4 all-gather.2
  23.8 68.3 all-gather.4
  230.5 10.2 reduce-scatter.1
where the time goes:
time: 250 us; the launch traced here: 247 us
  matrix products  103 us (41%)
  blocking collectives  45.9 us (18%)
  other arithmetic  36.6 us (15%)
  waiting for transfers between devices  24.2 us (10%)
  between operations  13.5 us (5%)
  local copies, waits for them, and re-layouts  12.9 us (5%)
  loops' own time  9.66 us (4%)
    all_gather x1, blocking collectives, shards(): lax.all_gather(key_rot, 'sp', axis=0, tiled=True)  33.7 us
    dot_general x12, matrix products, attend(): jnp.einsum('qhd,kd->hqk', query_rot, rot_block, preferred_element_type=jn...  22.3 us
    dot_general x12, matrix products, attend(): jnp.einsum('qhd,khd->hqk', queries, key_block, preferred_element_type=jnp...  19.1 us
    dot_general x12, matrix products, attend(): jnp.einsum('hqk,khd->qhd', exp_scores.astype(jnp.bfloat16), value_block,...  16.9 us
    dot_general x12, matrix products, expand_latent(): jnp.dot(lat_block, key_up, preferred_element_type=jnp.float32)  16.6 us
    dot_general x12, matrix products, expand_latent(): jnp.dot(lat_block, value_up, preferred_element_type=jnp.float32)  15.6 us
    reduce_sum x1, other arithmetic, shards(): jnp.sum(conv_out, axis=1)  14.7 us
    reduce_sum x12, other arithmetic, attend(): run_sum = run_sum * shrink + jnp.sum(exp_scores, axis=2)  13.1 us
  transfers between devices with their start and end apart: 4, of which 2 were waited for; matrix products, arithmetic and copies ran while one was open for 10% of the time, Pallas kernels for 0%

commit v1 on v0

v1 whole, which is shorter than its diff:
```python
import functools
import math

import jax
import jax.numpy as jnp
from jax import lax
from jax.experimental import pallas as pl
from jax.experimental.pallas import tpu as pltpu
from jax.sharding import PartitionSpec as P

D_MODEL = 2048
NOPE_DIM = 64
ROT_DIM = 32
VALUE_DIM = 64
CONV_CH = 1024
KERNEL = 31
ATT_WIDTH = 1024

norm_eps = 1e-06
far_below = -1e30
rope_base = 10000.0
SUM_ROWS = 16


def rotary_tables(positions, half_dim):
    frequency = rope_base ** (-jnp.arange(half_dim, dtype=jnp.float32) / half_dim)
    angles = positions.astype(jnp.float32)[:, None] * frequency[None, :]
    return (jnp.cos(angles), jnp.sin(angles))


def rotate_half(values, cos_table, sine_table):
    half_dim = cos_table.shape[-1]
    front_half = values[..., :half_dim]
    back_half = values[..., half_dim:]
    return jnp.concatenate(
        [
            front_half * cos_table - back_half * sine_table,
            back_half * cos_table + front_half * sine_table,
        ],
        axis=-1,
    )


def shift_by(block, axis, distance):
    devices = range(lax.axis_size(axis))
    return lax.ppermute(block, axis, [(i, i + distance) for i in devices if i + distance in devices])


def swap_bits(block, axis, bits):
    return lax.ppermute(block, axis, [(i, i ^ bits) for i in range(lax.axis_size(axis))])


def others(block, axis):
    size = lax.axis_size(axis)
    return [
        lax.ppermute(block, axis, [((i + d) % size, i) for i in range(size)])
        for d in range(1, size)
    ]


def total(block, axis):
    for part in others(block, axis):
        block = block + part
    return block


def in_order(mine, rest, axis, dim):
    size = 1 + len(rest)
    width = mine.shape[dim]
    ring = [mine] + rest + [mine] + rest[:-1]
    start = ((size - lax.axis_index(axis)) % size) * width
    return lax.dynamic_slice_in_dim(jnp.concatenate(ring, axis=dim), start, size * width, dim)


def attention_kernel(first, last, pieces, rows, groups, heads, vis_ref, *refs):
    refs = list(refs)
    qt_ref, qrt_ref, key_up_ref, value_up_ref = refs[:4]
    refs = refs[4:]
    slot_refs, refs = refs[:pieces], refs[pieces:]
    if first:
        (lat_ref, rot_ref), refs = refs[:2], refs[2:]
    else:
        (max_in, acc_in), refs = refs[:2], refs[2:]
    if last:
        (out_ref, max_ref, acc_ref, qbd_ref) = refs
    else:
        (max_ref, acc_ref, qbd_ref) = refs
    step = pl.program_id(0)
    pairs = heads // 2
    queries = qt_ref.shape[1]

    @pl.when(step == 0)
    def start():
        qbd_ref[...] = jnp.zeros_like(qbd_ref)
        for pair in range(pairs):
            for side in range(2):
                head = 2 * pair + side
                columns = slice(side * queries, (side + 1) * queries)
                qbd_ref[pair, side * NOPE_DIM : (side + 1) * NOPE_DIM, columns] = qt_ref[
                    head * NOPE_DIM : (head + 1) * NOPE_DIM, :
                ]
                qbd_ref[pair, 2 * NOPE_DIM : 2 * NOPE_DIM + ROT_DIM, columns] = qrt_ref[
                    head * ROT_DIM : (head + 1) * ROT_DIM, :
                ]
        if first:
            max_ref[...] = jnp.full_like(max_ref, far_below)
            acc_ref[...] = jnp.zeros_like(acc_ref)
        else:
            max_ref[...] = max_in[...]
            acc_ref[...] = acc_in[...]

    def visit(lat, rot, masked):
        count = lat.shape[0]
        keys = jnp.dot(lat, key_up_ref[...], preferred_element_type=jnp.float32).astype(jnp.bfloat16)
        values = lax.dot_general(
            value_up_ref[...], lat, (((1,), (1,)), ((), ())), preferred_element_type=jnp.float32
        ).astype(jnp.bfloat16)
        ones = jnp.ones((SUM_ROWS, count), jnp.bfloat16)
        if masked:
            visible = lax.broadcasted_iota(jnp.int32, (count, queries), 0) <= lax.broadcasted_iota(
                jnp.int32, (count, queries), 1
            )
        for pair in range(pairs):
            key_pair = jnp.concatenate(
                [keys[:, pair * 2 * NOPE_DIM : (pair + 1) * 2 * NOPE_DIM], rot], axis=1
            )
            scores = jnp.dot(key_pair, qbd_ref[pair], preferred_element_type=jnp.float32)
            for side in range(2):
                head = 2 * pair + side
                score = scores[:, side * queries : (side + 1) * queries]
                if masked:
                    score = jnp.where(visible, score, far_below)
                old_max = max_ref[head : head + 1, :]
                new_max = jnp.maximum(old_max, jnp.max(score, axis=0, keepdims=True))
                weights = jnp.exp2(score - new_max).astype(jnp.bfloat16)
                shrink = jnp.exp2(old_max - new_max)
                head_values = jnp.concatenate(
                    [values[head * VALUE_DIM : (head + 1) * VALUE_DIM, :], ones], axis=0
                )
                acc_ref[head] = acc_ref[head] * shrink + jnp.dot(
                    head_values, weights, preferred_element_type=jnp.float32
                )
                max_ref[head : head + 1, :] = new_max

    def from_slots():
        lats, rots = [], []
        for ref in slot_refs:
            lats.append(ref[0, :rows, :])
            packed = ref[0, rows:, :].astype(jnp.float32)[: rows // groups]
            rots += [packed[:, g * ROT_DIM : (g + 1) * ROT_DIM] for g in range(groups)]
        lat = jnp.concatenate(lats, axis=0)
        rot = jnp.concatenate(rots, axis=0)
        rot = jnp.concatenate(
            [rot, jnp.zeros((rot.shape[0], 128 - ROT_DIM), jnp.float32)], axis=1
        ).astype(jnp.bfloat16)
        visit(lat, rot, False)

    if first:

        @pl.when(step == 0)
        def own():
            visit(lat_ref[...], rot_ref[...], True)

        @pl.when((step > 0) & (vis_ref[jnp.maximum(step - 1, 0)] > 0))
        def slot():
            from_slots()

    else:

        @pl.when(vis_ref[step] > 0)
        def slot():
            from_slots()

    if last:

        @pl.when(step == pl.num_programs(0) - 1)
        def finish():
            for pair in range(pairs):
                both = jnp.concatenate(
                    [
                        acc_ref[2 * pair + side, :VALUE_DIM, :]
                        / acc_ref[2 * pair + side, VALUE_DIM : VALUE_DIM + 1, :]
                        for side in range(2)
                    ],
                    axis=0,
                )
                out_ref[:, pair * 2 * VALUE_DIM : (pair + 1) * 2 * VALUE_DIM] = both.T.astype(
                    out_ref.dtype
                )


def attention_stage(visible, queries_t, query_rot_t, key_up, value_up_t, slots, rows, groups,
                    own=None, state=None, last=False):
    first = own is not None
    heads = key_up.shape[1] // NOPE_DIM
    tok_rows = queries_t.shape[1]
    count = slots[0].shape[0]
    whole = lambda a: pl.BlockSpec(a.shape, lambda i, v: (0,) * a.ndim)
    if first:
        slot_map = lambda i, v: (jnp.maximum(i - 1, 0), 0, 0)
        extra = own
    else:
        slot_map = lambda i, v: (i, 0, 0)
        extra = state
    consts = [queries_t, query_rot_t, key_up, value_up_t]
    acc_shape = (heads, VALUE_DIM + SUM_ROWS, tok_rows)
    max_shape = (heads, tok_rows)
    qbd = pltpu.VMEM((heads // 2, 256, 2 * tok_rows), jnp.bfloat16)
    if last:
        out_shape = jax.ShapeDtypeStruct((tok_rows, heads * VALUE_DIM), jnp.bfloat16)
        out_specs = pl.BlockSpec(out_shape.shape, lambda i, v: (0, 0))
        scratch = [pltpu.VMEM(max_shape, jnp.float32), pltpu.VMEM(acc_shape, jnp.float32), qbd]
    else:
        out_shape = (
            jax.ShapeDtypeStruct(max_shape, jnp.float32),
            jax.ShapeDtypeStruct(acc_shape, jnp.float32),
        )
        out_specs = tuple(pl.BlockSpec(s.shape, lambda i, v, n=len(s.shape): (0,) * n) for s in out_shape)
        scratch = [qbd]
    flops = 2 * count * tok_rows * tok_rows * heads * (256 + VALUE_DIM)
    return pl.pallas_call(
        functools.partial(attention_kernel, first, last, len(slots), rows, groups, heads),
        grid_spec=pltpu.PrefetchScalarGridSpec(
            num_scalar_prefetch=1,
            grid=(count + (1 if first else 0),),
            in_specs=[whole(a) for a in consts]
            + [pl.BlockSpec((1,) + s.shape[1:], slot_map) for s in slots]
            + [whole(a) for a in extra],
            out_specs=out_specs,
            scratch_shapes=scratch,
        ),
        out_shape=out_shape,
        compiler_params=pltpu.CompilerParams(
            dimension_semantics=("arbitrary",), vmem_limit_bytes=48 * 1024 * 1024
        ),
        cost_estimate=pl.CostEstimate(
            flops=flops, bytes_accessed=4 << 20, transcendentals=count * tok_rows * tok_rows * heads
        ),
        name="attention_first" if first else "attention_rest",
    )(visible, *consts, *slots, *extra)


def conv_kernel(rim, gated_ref, rim_ref, taps_ref, out_ref, padded_ref):
    rows, chans = gated_ref.shape
    padded_ref[:rim, :] = rim_ref[...].astype(jnp.float32)
    padded_ref[rim : rim + rows, :] = gated_ref[...].astype(jnp.float32)
    offset = rim - (KERNEL - 1)
    step = math.gcd(rows, 64)
    for lane in range(0, chans, 128):
        lanes = slice(lane, lane + 128)
        for row in range(0, rows, step):
            acc = jnp.zeros((step, 128), jnp.float32)
            for phase in range(8):
                taps = range(phase, KERNEL, 8)
                start = row + offset + phase
                part = padded_ref[start : start + step + 8 * (len(taps) - 1), lanes]
                for j, tap in enumerate(taps):
                    acc = acc + taps_ref[tap : tap + 1, lanes] * part[8 * j : 8 * j + step]
            out_ref[row : row + step, lanes] = acc


def convolve(gated, rim, taps):
    rows, chans = gated.shape
    rim_rows = rim.shape[0]
    return pl.pallas_call(
        functools.partial(conv_kernel, rim_rows),
        out_shape=jax.ShapeDtypeStruct((rows, chans), jnp.float32),
        scratch_shapes=[pltpu.VMEM((rim_rows + rows, chans), jnp.float32)],
        cost_estimate=pl.CostEstimate(
            flops=2 * KERNEL * rows * chans * 50, bytes_accessed=6 * rows * chans, transcendentals=0
        ),
        name="conv",
    )(gated, rim, taps)


def shards(
    tokens,
    input_gain,
    query_weight,
    query_rot_weight,
    kv_down,
    rot_down,
    kv_gain,
    key_up,
    value_up,
    conv_value_weight,
    conv_gate_weight,
    conv_taps,
    conv_ln_gain,
    conv_ln_bias,
    att_out_gain,
    conv_out_gain,
    att_out_weight,
    conv_out_weight,
):
    tok_rows = tokens.shape[0]
    heads_here = key_up.shape[1] // NOPE_DIM
    tp_size, sp_size = lax.axis_size("tp"), lax.axis_size("sp")
    tp_index, sp_index = lax.axis_index("tp"), lax.axis_index("sp")
    f32, bf16 = jnp.float32, jnp.bfloat16

    wide = in_order(tokens, others(tokens, "tp"), "tp", 1).astype(f32)
    scaled = (wide * input_gain[None, :]).astype(bf16)
    row_scale = lax.rsqrt(jnp.sum(wide * wide, axis=1) / D_MODEL + norm_eps)[:, None]
    positions = sp_index * tok_rows + jnp.arange(tok_rows, dtype=jnp.int32)
    cos_table, sine_table = rotary_tables(positions, ROT_DIM // 2)

    def project(weight):
        return jnp.dot(scaled, weight, preferred_element_type=f32)

    latent_raw = project(kv_down)
    latent = (
        latent_raw
        * lax.rsqrt(jnp.mean(latent_raw * latent_raw, axis=1, keepdims=True) + norm_eps)
        * kv_gain[None, :]
    ).astype(bf16)
    key_rot = rotate_half(project(rot_down) * row_scale, cos_table, sine_table).astype(bf16)

    rows = tok_rows // tp_size
    rank = latent.shape[1]
    groups = max(
        g for g in range(1, rank // ROT_DIM + 1) if rows % g == 0 and (rows // g) % 8 == 0
    )
    my_lat = lax.dynamic_slice_in_dim(latent, tp_index * rows, rows, 0)
    my_rot = lax.dynamic_slice_in_dim(key_rot, tp_index * rows, rows, 0)
    packed = (
        my_rot.reshape(groups, rows // groups, ROT_DIM)
        .transpose(1, 0, 2)
        .reshape(rows // groups, groups * ROT_DIM)
    )
    packed = jnp.pad(
        packed, ((0, -(rows // groups) % 16), (0, rank - groups * ROT_DIM))
    )
    mine = jnp.concatenate([my_lat, packed], axis=0)

    plane = 4 if sp_size % 4 == 0 else 1
    high, low = sp_index // plane, sp_index % plane
    far = range(1, sp_size // plane)
    near_sent = [swap_bits(mine, "sp", b) for b in range(1, plane)]
    column = [shift_by(mine, "sp", plane * s) for s in far]
    near_vis = [((low ^ b) < low).astype(jnp.int32) for b in range(1, plane)]
    column_vis = [(high >= s).astype(jnp.int32) for s in far]
    slots_one = jnp.stack(near_sent + column)
    vis_one = jnp.stack(near_vis + column_vis)
    slots_one = [slots_one] + others(slots_one, "tp")
    if plane == 4:
        column_all = jnp.stack(column)
        rest = [swap_bits(column_all, "sp", 1), swap_bits(column_all, "sp", 2)]
        rest.append(jnp.stack([shift_by(near_sent[2], "sp", plane * s) for s in far]))
        slots_two = jnp.concatenate(rest, axis=0)
        vis_two = jnp.stack(column_vis * 3)
        slots_two = [slots_two] + others(slots_two, "tp")

    gated = (project(conv_value_weight) * row_scale * jax.nn.sigmoid(project(conv_gate_weight) * row_scale)).astype(bf16)
    rim_rows = 32
    rim = shift_by(gated[tok_rows - rim_rows :], "sp", 1)
    conv_out = convolve(gated, rim, conv_taps)
    moments = total(jnp.stack([jnp.sum(conv_out, axis=1), jnp.sum(conv_out * conv_out, axis=1)]), "tp")
    mean_val = moments[0] / CONV_CH
    spread = moments[1] / CONV_CH - mean_val * mean_val
    normed = (conv_out - mean_val[:, None]) * lax.rsqrt(spread + norm_eps)[:, None]
    swished = jax.nn.silu(normed * conv_ln_gain[None, :] + conv_ln_bias[None, :])
    conv_sq = total(jnp.sum(swished * swished, axis=1)[None, :], "tp")[0]
    conv_mixed = (
        swished * lax.rsqrt(conv_sq / CONV_CH + norm_eps)[:, None] * conv_out_gain[None, :]
    ).astype(bf16)
    conv_part = jnp.dot(conv_mixed, conv_out_weight, preferred_element_type=f32)

    query_scale = row_scale * (math.log2(math.e) / math.sqrt(NOPE_DIM + ROT_DIM))
    queries_t = (project(query_weight) * query_scale).astype(bf16).T
    query_rot_t = (
        rotate_half(
            (project(query_rot_weight) * query_scale).reshape(tok_rows, heads_here, ROT_DIM),
            cos_table[:, None, :],
            sine_table[:, None, :],
        )
        .astype(bf16)
        .reshape(tok_rows, heads_here * ROT_DIM)
        .T
    )
    value_up_t = value_up.T
    own = (latent, jnp.pad(key_rot, ((0, 0), (0, 128 - ROT_DIM))))
    stage = functools.partial(
        attention_stage,
        queries_t=queries_t,
        query_rot_t=query_rot_t,
        key_up=key_up,
        value_up_t=value_up_t,
        rows=rows,
        groups=groups,
    )
    if plane == 4:
        state = stage(vis_one, slots=slots_one, own=own)
        attended = stage(vis_two, slots=slots_two, state=state, last=True)
    else:
        attended = stage(vis_one, slots=slots_one, own=own, last=True)

    attended = attended.astype(f32)
    att_sq = total(jnp.sum(attended * attended, axis=1)[None, :], "tp")[0]
    att_part = jnp.dot(
        (attended * att_out_gain[None, :]).astype(bf16), att_out_weight, preferred_element_type=f32
    )
    partial = (att_part * lax.rsqrt(att_sq / ATT_WIDTH + norm_eps)[:, None] + conv_part).astype(bf16)
    width = D_MODEL // tp_size
    mixed = lax.dynamic_slice_in_dim(partial, tp_index * width, width, 1).astype(f32)
    for d in range(1, tp_size):
        target = (tp_index + tp_size - d) % tp_size
        send = lax.dynamic_slice_in_dim(partial, target * width, width, 1)
        mixed = mixed + lax.ppermute(
            send, "tp", [((i + d) % tp_size, i) for i in range(tp_size)]
        ).astype(f32)
    return mixed.astype(bf16)


def solution(mesh):
    return jax.shard_map(
        shards,
        mesh=mesh,
        in_specs=(
            P("sp", "tp"),
            P(),
            P(None, "tp"),
            P(None, "tp"),
            P(),
            P(),
            P(),
            P(None, "tp"),
            P(None, "tp"),
            P(None, "tp"),
            P(None, "tp"),
            P(None, "tp"),
            P("tp"),
            P("tp"),
            P("tp"),
            P("tp"),
            P("tp", None),
            P("tp", None),
        ),
        out_specs=P("sp", "tp"),
        check_vma=False,
    )
```

time: 250 us -> 127 us (0.51)
  matrix products: 103 us -> 10.2 us
  Pallas kernels: 0 us -> 47.7 us
  blocking collectives: 45.9 us -> 0 us
  other arithmetic: 36.6 us -> 9.26 us
  starting transfers between devices: 1.51 us -> 22.6 us
  between operations: 13.5 us -> 0.62 us
  loops' own time: 9.66 us -> 0 us
  waiting for transfers between devices: 24.2 us -> 19.3 us
  local copies, waits for them, and re-layouts: 12.9 us -> 16.7 us
    dot_general x68 -> x8, matrix products: 103 us -> 10.2 us  [the longest x6 7.98 us: project(): return jnp.dot(scaled, weight, preferred_element_type=f32)]
    pallas_call x0 -> x3, Pallas kernels: none -> 47.7 us  [the longest x2 42.5 us: attention_stage(): pl.pallas_call(functools.partial(attention_kernel, first, last, len(slots...]
    all_gather x1 -> x0, blocking collectives: 33.7 us -> none  [shards(): lax.all_gather(key_rot, 'sp', axis=0, tiled=True)]
    ppermute x1 -> x19, starting transfers between devices: 1.42 us -> 22.6 us  [the longest x7 9.19 us: shift_by(): lax.ppermute(block, axis, [(i, i + distance) for i in devices if i + dist...]
    ppermute x1 -> x19, waiting for transfers between devices: 0.01 us -> 19.3 us  [the longest x7 15.4 us: shift_by(): lax.ppermute(block, axis, [(i, i + distance) for i in devices if i + dist...]
    reduce_sum x15 -> x3, other arithmetic: 17 us -> 3.04 us  [the longest x1 2.41 us: shards(): jnp.sum(wide * wide, axis=1) / D_MODEL + norm_eps]
    reduce_sum x1, other arithmetic: 14.7 us -> 1.31 us  [shards(): jnp.sum(conv_out, axis=1)]
    all_gather x2 -> x0, waiting for transfers between devices: 13 us -> none  [the longest x1 13 us: shards(): lax.all_gather(tokens, 'tp', axis=1, tiled=True).astype(jnp.float32)]
  transfers between devices with their start and end apart: 4 -> 19, of which waited for: 2 -> 7; matrix products, arithmetic and copies ran while one was open for 10% -> 15% of each run, Pallas kernels for 0% -> 19%
where the time goes in v1:
time: 127 us; the launch traced here: 126 us
  Pallas kernels  47.7 us (38%)
  starting transfers between devices  22.6 us (18%)
  waiting for transfers between devices  19.3 us (15%)
  local copies, waits for them, and re-layouts  16.7 us (13%)
  matrix products  10.2 us (8%)
  other arithmetic  9.26 us (7%)
    pallas_call x2, Pallas kernels, attention_stage(): pl.pallas_call(functools.partial(attention_kernel, first, last, len(slots...  42.5 us
    ppermute x7, waiting for transfers between devices, shift_by(): lax.ppermute(block, axis, [(i, i + distance) for i in devices if i + dist...  15.4 us
    unnamed x68, local copies, waits for them, and re-layouts  13 us
    ppermute x7, starting transfers between devices, shift_by(): lax.ppermute(block, axis, [(i, i + distance) for i in devices if i + dist...  9.19 us
    dot_general x6, matrix products, project(): return jnp.dot(scaled, weight, preferred_element_type=f32)  7.98 us
    ppermute x5, starting transfers between devices, swap_bits(): lax.ppermute(block, axis, [(i, i ^ bits) for i in range(lax.axis_size(axi...  7.08 us
    ppermute x6, starting transfers between devices, others(): lax.ppermute(block, axis, [((i + d) % size, i) for i in range(size)])  6.16 us
    pallas_call x1, Pallas kernels, convolve(): pl.pallas_call(functools.partial(conv_kernel, rim_rows), out_shape=jax.Sh...  5.17 us
  transfers between devices with their start and end apart: 19, of which 7 were waited for; matrix products, arithmetic and copies ran while one was open for 15% of the time, Pallas kernels for 19%

profile of v1, /device:TPU:31, one launch (start us, length us, event | category | flops | bytes accessed | tf_op | source)
XLA Modules:
  0.0 126.3 jit_solution(8286898491428923368)
XLA Ops:
  2.9 2.4 %fusion.1 = (f32[384]{0:T(512)S(1)}, bf16[384,2048]{1,0:T(8,128)(2,1)S(1)}) fusion(s32[]{:T(128)S(6)} %select_n.34, bf16[384,1024]{1,0:T(8,128)(2,1)} %param.18, bf16[384,1024]{1,0:T(8,128)(2,1)S(1)} %collective-permute-done), kind=kLoop, calls=%fused_computation.3 | loop fusion | flops 7077504 | bytes 3147268 | tf_op jit(solution)/shard_map/reduce_sum | solution.py:304
  7.7 2.5 %multiply_reduce_fusion.2 = (f32[384]{0:T(512)S(1)}, f32[384,256]{1,0:T(8,128)S(1)}) fusion(bf16[2048,256]{1,0:T(8,128)(2,1)} %param.22, bf16[384,2048]{1,0:T(8,128)(2,1)} %copy-done.8, f32[2048]{0:T(1024)S(1)} %copy-done.27), kind=kOutput, calls=%fused_computation.38 | convolution fusion | flops 405208704 | bytes 3024384 | tf_op jit(solution)/shard_map/dot_general | solution.py:309
  11.5 1.3 %collective-permute-start.1 = (bf16[224,256]{1,0:T(8,128)(2,1)}, bf16[224,256]{1,0:T(8,128)(2,1)S(1)}, u32[]{:S(2)}, u32[]{:S(2)}) collective-permute-start(bf16[224,256]{1,0:T(8,128)(2,1)} %fusion.27), channel_id=1, source_target_pairs={{0,8},{2,10},{4,12},{6,14},{8,16},{10,18},{12,20},{14,22},{16,24},... | collective-permute-start | bytes 344072 | tf_op jit(solution)/shard_map/ppermute | solution.py:46
  12.8 1.3 %collective-permute-start.2 = (bf16[224,256]{1,0:T(8,128)(2,1)}, bf16[224,256]{1,0:T(8,128)(2,1)S(1)}, u32[]{:S(2)}, u32[]{:S(2)}) collective-permute-start(bf16[224,256]{1,0:T(8,128)(2,1)} %fusion.27), channel_id=1, source_target_pairs={{0,16},{2,18},{4,20},{6,22},{8,24},{10,26},{12,28},{14,30},{1,17},... | collective-permute-start | bytes 344072 | tf_op jit(solution)/shard_map/ppermute | solution.py:46
  14.9 2.0 %fusion.11.refs_0_ = bf16[512,384]{1,0:T(8,128)(2,1)} fusion(bf16[2048,512]{1,0:T(8,128)(2,1)S(1)} %copy-done.21, bf16[384,2048]{1,0:T(8,128)(2,1)S(1)} %copy-done.9, f32[2048]{0:T(1024)S(1)} %copy-done.27, f32[384]{0:T(512)S(1)} %get-tuple-element.21), kind=kOutput, calls=%fused_computation.21 | convolution fusion | flops 808058880 | bytes 4072960 | tf_op jit(solution)/shard_map/dot_general | solution.py:309
  19.6 1.3 %collective-permute-start.15 = (bf16[32,512]{1,0:T(8,128)(2,1)S(1)}, bf16[32,512]{1,0:T(8,128)(2,1)S(1)}, u32[]{:S(2)}, u32[]{:S(2)}) collective-permute-start(bf16[32,512]{1,0:T(8,128)(2,1)S(1)} %slice.32), channel_id=1, source_target_pairs={{0,2},{2,4},{4,6},{6,8},{8,10},{10,12},{12,14},{14,16},{16,18},{18... | collective-permute-start | bytes 98312 | tf_op jit(solution)/shard_map/ppermute | solution.py:46
  21.0 3.3 %collective-permute-done.15.rim_ref = bf16[32,512]{1,0:T(8,128)(2,1)S(1)} collective-permute-done((bf16[32,512]{1,0:T(8,128)(2,1)S(1)}, bf16[32,512]{1,0:T(8,128)(2,1)S(1)}, u32[]{:S(2)}, u32[]{:S(2)}) %collective-permute-start.15) | collective-permute-done | bytes 32800 | tf_op jit(solution)/shard_map/ppermute | solution.py:46
  24.9 5.2 %conv.1 = f32[384,512]{1,0:T(8,128)} custom-call(bf16[384,512]{1,0:T(8,128)(2,1)} %copy-done.14, bf16[32,512]{1,0:T(8,128)(2,1)} %copy-done.26, f32[31,512]{1,0:T(8,128)} %taps_ref.1), custom_call_target="tpu_custom_call" | custom-call | flops 609484800 | bytes 1179648 | tf_op jit(solution)/shard_map/conv/pallas_call | solution.py:265
  30.0 1.3 %fusion.32 = (f32[384]{0:T(512)S(1)}, f32[384]{0:T(512)S(1)}) fusion(f32[384,512]{1,0:T(8,128)} %conv.1), kind=kLoop, calls=%fused_computation.81 | loop fusion | flops 589056 | bytes 789504 | tf_op jit(solution)/shard_map/reduce_sum | solution.py:358
  31.4 2.1 %collective-permute-start.16 = (f32[2,384]{1,0:T(2,128)S(1)}, f32[2,384]{1,0:T(2,128)S(1)}, u32[]{:S(2)}, u32[]{:S(2)}) collective-permute-start(f32[2,384]{1,0:T(2,128)S(1)} %pad_maximum_fusion.3), channel_id=1, source_target_pairs={{1,0},{0,1},{3,2},{2,3},{5,4},{4,5},{7,6},{6,7},{9,8},{8,9},{11,10... | collective-permute-start | bytes 9224 | tf_op jit(solution)/shard_map/ppermute | solution.py:56
  34.3 1.3 %collective-permute-start.3 = (bf16[224,256]{1,0:T(8,128)(2,1)}, bf16[224,256]{1,0:T(8,128)(2,1)S(1)}, u32[]{:S(2)}, u32[]{:S(2)}) collective-permute-start(bf16[224,256]{1,0:T(8,128)(2,1)} %fusion.27), channel_id=1, source_target_pairs={{0,24},{2,26},{4,28},{6,30},{1,25},{3,27},{5,29},{7,31}} | collective-permute-start | bytes 344072 | tf_op jit(solution)/shard_map/ppermute | solution.py:46
  35.7 4.0 %collective-permute-start.6 = (bf16[224,256]{1,0:T(8,128)(2,1)}, bf16[224,256]{1,0:T(8,128)(2,1)S(1)}, u32[]{:S(2)}, u32[]{:S(2)}) collective-permute-start(bf16[224,256]{1,0:T(8,128)(2,1)} %fusion.27), channel_id=1, source_target_pairs={{0,6},{2,4},{4,2},{6,0},{8,14},{10,12},{12,10},{14,8},{16,22},{18,... | collective-permute-start | bytes 344072 | tf_op jit(solution)/shard_map/ppermute | solution.py:50
  39.7 4.6 %collective-permute-done.3 = bf16[224,256]{1,0:T(8,128)(2,1)S(1)} collective-permute-done((bf16[224,256]{1,0:T(8,128)(2,1)}, bf16[224,256]{1,0:T(8,128)(2,1)S(1)}, u32[]{:S(2)}, u32[]{:S(2)}) %collective-permute-start.3) | collective-permute-done | bytes 114720 | tf_op jit(solution)/shard_map/ppermute | solution.py:46
  44.4 2.2 %collective-permute-start.4 = (bf16[3,224,256]{2,1,0:T(8,128)(2,1)S(1)}, bf16[3,224,256]{2,1,0:T(8,128)(2,1)S(1)}, u32[]{:S(2)}, u32[]{:S(2)}) collective-permute-start(bf16[3,224,256]{2,1,0:T(8,128)(2,1)S(1)} %pad_maximum_fusion), channel_id=1, source_target_pairs={{0,2},{2,0},{4,6},{6,4},{8,10},{10,8},{12,14},{14,12},{16,18},{18,... | collective-permute-start | bytes 1032200 | tf_op jit(solution)/shard_map/ppermute | solution.py:50
  50.6 1.8 %collective-permute-start.13 = (bf16[6,224,256]{2,1,0:T(8,128)(2,1)S(1)}, bf16[6,224,256]{2,1,0:T(8,128)(2,1)}, u32[]{:S(2)}, u32[]{:S(2)}) collective-permute-start(bf16[6,224,256]{2,1,0:T(8,128)(2,1)S(1)} %constant_dynamic-update-slice_fusion.2.refs_4_), channel_id=1, source_target_pairs={{1,0},{0,1},{3,2},{2,3},{5,4},{4,5},{7,6},{6,7},{9,8},{8,9},{11,10... | collective-permute-start | bytes 2064392 | tf_op jit(solution)/shard_map/ppermute | solution.py:56
  52.4 1.3 %collective-permute-start.7 = (bf16[224,256]{1,0:T(8,128)(2,1)S(1)}, bf16[224,256]{1,0:T(8,128)(2,1)S(1)}, u32[]{:S(2)}, u32[]{:S(2)}) collective-permute-start(bf16[224,256]{1,0:T(8,128)(2,1)S(1)} %collective-permute-done.6), channel_id=1, source_target_pairs={{0,8},{2,10},{4,12},{6,14},{8,16},{10,18},{12,20},{14,22},{16,24},... | collective-permute-start | bytes 344072 | tf_op jit(solution)/shard_map/ppermute | solution.py:46
  53.7 1.3 %collective-permute-start.8 = (bf16[224,256]{1,0:T(8,128)(2,1)S(1)}, bf16[224,256]{1,0:T(8,128)(2,1)S(1)}, u32[]{:S(2)}, u32[]{:S(2)}) collective-permute-start(bf16[224,256]{1,0:T(8,128)(2,1)S(1)} %collective-permute-done.6), channel_id=1, source_target_pairs={{0,16},{2,18},{4,20},{6,22},{8,24},{10,26},{12,28},{14,30},{1,17},... | collective-permute-start | bytes 344072 | tf_op jit(solution)/shard_map/ppermute | solution.py:46
  55.0 1.5 %collective-permute-start.9 = (bf16[224,256]{1,0:T(8,128)(2,1)S(1)}, bf16[224,256]{1,0:T(8,128)(2,1)S(1)}, u32[]{:S(2)}, u32[]{:S(2)}) collective-permute-start(bf16[224,256]{1,0:T(8,128)(2,1)S(1)} %collective-permute-done.6), channel_id=1, source_target_pairs={{0,24},{2,26},{4,28},{6,30},{1,25},{3,27},{5,29},{7,31}} | collective-permute-start | bytes 344072 | tf_op jit(solution)/shard_map/ppermute | solution.py:46
  59.7 6.5 %collective-permute-done.8 = bf16[224,256]{1,0:T(8,128)(2,1)S(1)} collective-permute-done((bf16[224,256]{1,0:T(8,128)(2,1)S(1)}, bf16[224,256]{1,0:T(8,128)(2,1)S(1)}, u32[]{:S(2)}, u32[]{:S(2)}) %collective-permute-start.8) | collective-permute-done | bytes 114720 | tf_op jit(solution)/shard_map/ppermute | solution.py:46
  73.7 18.6 %attention_first.1 = (f32[8,384]{1,0:T(8,128)S(1)}, f32[8,80,384]{2,1,0:T(8,128)S(1)}) custom-call(s32[6]{0:T(128)S(1)} %stack.116.vis_ref, bf16[512,384]{1,0:T(8,128)(2,1)S(1)} %copy-done.3, bf16[256,384]{1,0:T(8,128)(2,1)S(1)} %bitcast.44, bf16[256,512]{1,0:T(8,128)(2,1)S(1)} %copy-done.1, bf16[512,256]{1,0:T(8,128)(2,1)S(1)} %bitcast.42, ...), custom_call_target="tpu_custom_call" | custom-call | flops 4529848320 | bytes 4194304 | tf_op jit(solution)/shard_map/attention_first/pallas_call | solution.py:221
  92.3 23.9 %attention_rest.1 = bf16[384,512]{1,0:T(8,128)(2,1)S(1)} custom-call(s32[9]{0:T(128)S(1)} %stack.102.vis_ref, bf16[512,384]{1,0:T(8,128)(2,1)S(1)} %copy-done.3, bf16[256,384]{1,0:T(8,128)(2,1)S(1)} %bitcast.45, bf16[256,512]{1,0:T(8,128)(2,1)S(1)} %copy-done.2, bf16[512,256]{1,0:T(8,128)(2,1)S(1)} %bitcast.43, ...), custom_call_target="tpu_custom_call" | custom-call | flops 6794772480 | bytes 4194304 | tf_op jit(solution)/shard_map/attention_rest/pallas_call | solution.py:221
  117.1 1.2 fusion.21
  121.7 2.3 %collective-permute-done.18 = bf16[384,1024]{1,0:T(8,128)(2,1)S(1)} collective-permute-done((bf16[384,1024]{1,0:T(8,128)(2,1)}, bf16[384,1024]{1,0:T(8,128)(2,1)S(1)}, u32[]{:S(2)}, u32[]{:S(2)}) %collective-permute-start.18) | collective-permute-done | bytes 786464 | tf_op jit(solution)/shard_map/ppermute | solution.py:409
  124.0 2.3 %add_convert_fusion.1 = bf16[384,1024]{1,0:T(8,128)(2,1)} fusion(bf16[384,1024]{1,0:T(8,128)(2,1)S(1)} %collective-permute-done.18, bf16[384,2048]{1,0:T(8,128)(2,1)} %copy-done.4, s32[]{:T(128)S(6)} %select_n.37), kind=kLoop, calls=%fused_computation.10 | loop fusion | flops 1572864 | bytes 2359300 | tf_op jit(solution)/shard_map/convert_element_type | solution.py:412
  (132 shorter events, 30.1 us)
Async XLA Ops:
  0.0 117.1 %copy-start = (bf16[512,2048]{1,0:T(8,128)(2,1)S(1)}, bf16[512,2048]{1,0:T(8,128)(2,1)}, u32[]{:S(2)}) copy-start(bf16[512,2048]{1,0:T(8,128)(2,1)} %param.35) | copy-start | bytes 6291460
  0.0 2.9 %collective-permute-start = (bf16[384,1024]{1,0:T(8,128)(2,1)}, bf16[384,1024]{1,0:T(8,128)(2,1)S(1)}, u32[]{:S(2)}, u32[]{:S(2)}) collective-permute-start(bf16[384,1024]{1,0:T(8,128)(2,1)} %param.18), channel_id=1, source_target_pairs={{1,0},{0,1},{3,2},{2,3},{5,4},{4,5},{7,6},{6,7},{9,8},{8,9},{11,10... | collective-permute-start | bytes 2359304 | tf_op jit(solution)/shard_map/ppermute | solution.py:56
  11.0 35.9 %collective-permute-start.11 = (bf16[224,256]{1,0:T(8,128)(2,1)}, bf16[224,256]{1,0:T(8,128)(2,1)}, u32[]{:S(2)}, u32[]{:S(2)}) collective-permute-start(bf16[224,256]{1,0:T(8,128)(2,1)} %fusion.27), channel_id=1, source_target_pairs={{0,2},{2,0},{4,6},{6,4},{8,10},{10,8},{12,14},{14,12},{16,18},{18,... | collective-permute-start | bytes 344072 | tf_op jit(solution)/shard_map/ppermute | solution.py:50
  11.3 36.6 %collective-permute-start.12 = (bf16[224,256]{1,0:T(8,128)(2,1)}, bf16[224,256]{1,0:T(8,128)(2,1)}, u32[]{:S(2)}, u32[]{:S(2)}) collective-permute-start(bf16[224,256]{1,0:T(8,128)(2,1)} %fusion.27), channel_id=1, source_target_pairs={{0,4},{2,6},{4,0},{6,2},{8,12},{10,14},{12,8},{14,10},{16,20},{18,... | collective-permute-start | bytes 344072 | tf_op jit(solution)/shard_map/ppermute | solution.py:50
  11.5 24.1 %collective-permute-start.1 = (bf16[224,256]{1,0:T(8,128)(2,1)}, bf16[224,256]{1,0:T(8,128)(2,1)S(1)}, u32[]{:S(2)}, u32[]{:S(2)}) collective-permute-start(bf16[224,256]{1,0:T(8,128)(2,1)} %fusion.27), channel_id=1, source_target_pairs={{0,8},{2,10},{4,12},{6,14},{8,16},{10,18},{12,20},{14,22},{16,24},... | collective-permute-start | bytes 344072 | tf_op jit(solution)/shard_map/ppermute | solution.py:46
  12.8 26.9 %collective-permute-start.2 = (bf16[224,256]{1,0:T(8,128)(2,1)}, bf16[224,256]{1,0:T(8,128)(2,1)S(1)}, u32[]{:S(2)}, u32[]{:S(2)}) collective-permute-start(bf16[224,256]{1,0:T(8,128)(2,1)} %fusion.27), channel_id=1, source_target_pairs={{0,16},{2,18},{4,20},{6,22},{8,24},{10,26},{12,28},{14,30},{1,17},... | collective-permute-start | bytes 344072 | tf_op jit(solution)/shard_map/ppermute | solution.py:46
  19.6 4.7 %collective-permute-start.15 = (bf16[32,512]{1,0:T(8,128)(2,1)S(1)}, bf16[32,512]{1,0:T(8,128)(2,1)S(1)}, u32[]{:S(2)}, u32[]{:S(2)}) collective-permute-start(bf16[32,512]{1,0:T(8,128)(2,1)S(1)} %slice.32), channel_id=1, source_target_pairs={{0,2},{2,4},{4,6},{6,8},{8,10},{10,12},{12,14},{14,16},{16,18},{18... | collective-permute-start | bytes 98312 | tf_op jit(solution)/shard_map/ppermute | solution.py:46
  31.4 3.0 %collective-permute-start.16 = (f32[2,384]{1,0:T(2,128)S(1)}, f32[2,384]{1,0:T(2,128)S(1)}, u32[]{:S(2)}, u32[]{:S(2)}) collective-permute-start(f32[2,384]{1,0:T(2,128)S(1)} %pad_maximum_fusion.3), channel_id=1, source_target_pairs={{1,0},{0,1},{3,2},{2,3},{5,4},{4,5},{7,6},{6,7},{9,8},{8,9},{11,10... | collective-permute-start | bytes 9224 | tf_op jit(solution)/shard_map/ppermute | solution.py:56
  33.5 34.8 %copy-start.5 = (f32[384,512]{1,0:T(8,128)S(1)}, f32[384,512]{1,0:T(8,128)}, u32[]{:S(2)}) copy-start(f32[384,512]{1,0:T(8,128)} %conv.1) | copy-start | bytes 2359300
  33.5 34.8 %copy-start.15 = (f32[512]{0:T(512)S(1)}, f32[512]{0:T(512)}, u32[]{:S(2)}) copy-start(f32[512]{0:T(512)} %param.31) | copy-start | bytes 6148
  33.6 34.8 %copy-start.17 = (f32[512]{0:T(512)S(1)}, f32[512]{0:T(512)}, u32[]{:S(2)}) copy-start(f32[512]{0:T(512)} %param.30) | copy-start | bytes 6148
  34.3 10.0 %collective-permute-start.3 = (bf16[224,256]{1,0:T(8,128)(2,1)}, bf16[224,256]{1,0:T(8,128)(2,1)S(1)}, u32[]{:S(2)}, u32[]{:S(2)}) collective-permute-start(bf16[224,256]{1,0:T(8,128)(2,1)} %fusion.27), channel_id=1, source_target_pairs={{0,24},{2,26},{4,28},{6,30},{1,25},{3,27},{5,29},{7,31}} | collective-permute-start | bytes 344072 | tf_op jit(solution)/shard_map/ppermute | solution.py:46
  35.7 13.1 %collective-permute-start.6 = (bf16[224,256]{1,0:T(8,128)(2,1)}, bf16[224,256]{1,0:T(8,128)(2,1)S(1)}, u32[]{:S(2)}, u32[]{:S(2)}) collective-permute-start(bf16[224,256]{1,0:T(8,128)(2,1)} %fusion.27), channel_id=1, source_target_pairs={{0,6},{2,4},{4,2},{6,0},{8,14},{10,12},{12,10},{14,8},{16,22},{18,... | collective-permute-start | bytes 344072 | tf_op jit(solution)/shard_map/ppermute | solution.py:50
  44.4 10.7 %collective-permute-start.4 = (bf16[3,224,256]{2,1,0:T(8,128)(2,1)S(1)}, bf16[3,224,256]{2,1,0:T(8,128)(2,1)S(1)}, u32[]{:S(2)}, u32[]{:S(2)}) collective-permute-start(bf16[3,224,256]{2,1,0:T(8,128)(2,1)S(1)} %pad_maximum_fusion), channel_id=1, source_target_pairs={{0,2},{2,0},{4,6},{6,4},{8,10},{10,8},{12,14},{14,12},{16,18},{18,... | collective-permute-start | bytes 1032200 | tf_op jit(solution)/shard_map/ppermute | solution.py:50
  46.5 10.7 %collective-permute-start.5 = (bf16[3,224,256]{2,1,0:T(8,128)(2,1)S(1)}, bf16[3,224,256]{2,1,0:T(8,128)(2,1)S(1)}, u32[]{:S(2)}, u32[]{:S(2)}) collective-permute-start(bf16[3,224,256]{2,1,0:T(8,128)(2,1)S(1)} %pad_maximum_fusion), channel_id=1, source_target_pairs={{0,4},{2,6},{4,0},{6,2},{8,12},{10,14},{12,8},{14,10},{16,20},{18,... | collective-permute-start | bytes 1032200 | tf_op jit(solution)/shard_map/ppermute | solution.py:50
  50.6 21.1 %collective-permute-start.13 = (bf16[6,224,256]{2,1,0:T(8,128)(2,1)S(1)}, bf16[6,224,256]{2,1,0:T(8,128)(2,1)}, u32[]{:S(2)}, u32[]{:S(2)}) collective-permute-start(bf16[6,224,256]{2,1,0:T(8,128)(2,1)S(1)} %constant_dynamic-update-slice_fusion.2.refs_4_), channel_id=1, source_target_pairs={{1,0},{0,1},{3,2},{2,3},{5,4},{4,5},{7,6},{6,7},{9,8},{8,9},{11,10... | collective-permute-start | bytes 2064392 | tf_op jit(solution)/shard_map/ppermute | solution.py:56
  52.4 6.6 %collective-permute-start.7 = (bf16[224,256]{1,0:T(8,128)(2,1)S(1)}, bf16[224,256]{1,0:T(8,128)(2,1)S(1)}, u32[]{:S(2)}, u32[]{:S(2)}) collective-permute-start(bf16[224,256]{1,0:T(8,128)(2,1)S(1)} %collective-permute-done.6), channel_id=1, source_target_pairs={{0,8},{2,10},{4,12},{6,14},{8,16},{10,18},{12,20},{14,22},{16,24},... | collective-permute-start | bytes 344072 | tf_op jit(solution)/shard_map/ppermute | solution.py:46
  53.7 12.4 %collective-permute-start.8 = (bf16[224,256]{1,0:T(8,128)(2,1)S(1)}, bf16[224,256]{1,0:T(8,128)(2,1)S(1)}, u32[]{:S(2)}, u32[]{:S(2)}) collective-permute-start(bf16[224,256]{1,0:T(8,128)(2,1)S(1)} %collective-permute-done.6), channel_id=1, source_target_pairs={{0,16},{2,18},{4,20},{6,22},{8,24},{10,26},{12,28},{14,30},{1,17},... | collective-permute-start | bytes 344072 | tf_op jit(solution)/shard_map/ppermute | solution.py:46
  55.0 11.8 %collective-permute-start.9 = (bf16[224,256]{1,0:T(8,128)(2,1)S(1)}, bf16[224,256]{1,0:T(8,128)(2,1)S(1)}, u32[]{:S(2)}, u32[]{:S(2)}) collective-permute-start(bf16[224,256]{1,0:T(8,128)(2,1)S(1)} %collective-permute-done.6), channel_id=1, source_target_pairs={{0,24},{2,26},{4,28},{6,30},{1,25},{3,27},{5,29},{7,31}} | collective-permute-start | bytes 344072 | tf_op jit(solution)/shard_map/ppermute | solution.py:46
  67.5 24.8 %collective-permute-start.10 = (bf16[9,224,256]{2,1,0:T(8,128)(2,1)}, bf16[9,224,256]{2,1,0:T(8,128)(2,1)}, u32[]{:S(2)}, u32[]{:S(2)}) collective-permute-start(bf16[9,224,256]{2,1,0:T(8,128)(2,1)} %bitcast_dynamic-update-slice_fusion.3.refs_4_), channel_id=1, source_target_pairs={{1,0},{0,1},{3,2},{2,3},{5,4},{4,5},{7,6},{6,7},{9,8},{8,9},{11,10... | collective-permute-start | bytes 3096584 | tf_op jit(solution)/shard_map/ppermute | solution.py:56
  69.5 1.5 %collective-permute-start.17 = (f32[1,384]{1,0:T(1,128)}, f32[1,384]{1,0:T(1,128)}, u32[]{:S(2)}, u32[]{:S(2)}) collective-permute-start(f32[1,384]{1,0:T(1,128)} %broadcast_in_dim.5), channel_id=1, source_target_pairs={{1,0},{0,1},{3,2},{2,3},{5,4},{4,5},{7,6},{6,7},{9,8},{8,9},{11,10... | collective-permute-start | bytes 4616 | tf_op jit(solution)/shard_map/ppermute | solution.py:56
  92.3 24.8 %copy-start.6 = (f32[384,512]{1,0:T(8,128)S(1)}, f32[384,512]{1,0:T(8,128)}, u32[]{:S(2)}) copy-start(f32[384,512]{1,0:T(8,128)} %conv.1) | copy-start | bytes 2359300
  116.5 1.8 %collective-permute-start.14 = (f32[1,384]{1,0:T(1,128)S(1)}, f32[1,384]{1,0:T(1,128)S(1)}, u32[]{:S(2)}, u32[]{:S(2)}) collective-permute-start(f32[1,384]{1,0:T(1,128)S(1)} %broadcast_in_dim.4), channel_id=1, source_target_pairs={{1,0},{0,1},{3,2},{2,3},{5,4},{4,5},{7,6},{6,7},{9,8},{8,9},{11,10... | collective-permute-start | bytes 4616 | tf_op jit(solution)/shard_map/ppermute | solution.py:56
  121.5 2.5 %collective-permute-start.18 = (bf16[384,1024]{1,0:T(8,128)(2,1)}, bf16[384,1024]{1,0:T(8,128)(2,1)S(1)}, u32[]{:S(2)}, u32[]{:S(2)}) collective-permute-start(bf16[384,1024]{1,0:T(8,128)(2,1)} %constant_dynamic-slice_fusion), channel_id=1, source_target_pairs={{1,0},{0,1},{3,2},{2,3},{5,4},{4,5},{7,6},{6,7},{9,8},{8,9},{11,10... | collective-permute-start | bytes 2359304 | tf_op jit(solution)/shard_map/ppermute | solution.py:409
  (24 other events, 184.1 us)
